TPU v7x, 32 devices: a whole 2x2x4 slice. The times are simulated.
32 devices in a mesh: fs: 8 (over z, x), tp: 4 (over y, core).
Axes of the slice: x: 2, y: 2, z: 4, core: 2. Of those that a mesh axis runs over, the one named last changes fastest.
Arguments:
- tokens: bfloat16 [1024, 2048], P('fs'), may hold values from -6 to 6
- route_ids: int32 [1024, 2], P('fs'), may hold values from 0 to 15, as said below
- route_weights: float32 [1024, 2], P('fs'), may hold values from 0.05 to 0.6
- norm_gain: float32 [2048], P('fs'), may hold values from 0.1 to 1.9
- gate_weight: float32 [16, 2048, 1024], P(None, 'fs', 'tp'), may hold values from -6 to 6
- up_weight: float32 [16, 2048, 1024], P(None, 'fs', 'tp'), may hold values from -6 to 6
- down_weight: float32 [16, 2048, 1024], P(None, 'fs', 'tp'), may hold values from -6 to 6
Outputs:
- gate_served: bfloat16 [16, 2048, 1024], P('fs', None, 'tp')
- up_served: bfloat16 [16, 2048, 1024], P('fs', None, 'tp')
- down_served: bfloat16 [16, 2048, 1024], P('fs', None, 'tp')
- combined: bfloat16 [1024, 2048], P('fs', 'tp')
Inputs may be any that keep to these rules, and one draw needn't show every extreme that they name: `route_ids`: each row names 2 different experts of one group, numbers g * 4 to g * 4 + 3 for some g. In each aligned block of 128 rows (the rows of one index of fs) no expert is named by more than 32 rows, and some experts are named by exactly 32 rows in every block.
All inputs are finite; a program needn't handle non-finite values.
Results may differ from a plain program's by a relative error of at most 0.015.
Values may be sent and summed in bfloat16 or wider, within the bound.
A program may use at most 64 MiB of HBM per device.

v0:
```python
import jax
import jax.numpy as jnp
from jax import lax
from jax.sharding import PartitionSpec as P

GROUPS = 4
epsilon = 1e-06


def body(tokens, route_ids, route_weights, norm_gain, gate_weight, up_weight, down_weight):
    scaling = norm_gain[:, None]
    gate_folded = (scaling * gate_weight).astype(jnp.bfloat16)
    up_folded = (scaling * up_weight).astype(jnp.bfloat16)
    down_rounded = down_weight.astype(jnp.bfloat16)
    gate_served, up_served, down_served = (
        lax.all_to_all(gate_folded, "fs", split_axis=0, concat_axis=1, tiled=True),
        lax.all_to_all(up_folded, "fs", split_axis=0, concat_axis=1, tiled=True),
        lax.all_to_all(down_rounded, "fs", split_axis=0, concat_axis=1, tiled=True),
    )
    widened = tokens.astype(jnp.float32)
    normed = (
        widened * lax.rsqrt(jnp.mean(widened * widened, axis=1, keepdims=True) + epsilon)
    ).astype(jnp.bfloat16)
    tok_rows, d_model = tokens.shape
    routes = route_ids.shape[1]
    experts = gate_weight.shape[0]
    sources = lax.axis_size("fs")
    per_device = experts // sources
    capacity = tok_rows * GROUPS // experts
    flat_ids = route_ids.reshape(-1)
    onehot = (flat_ids[:, None] == jnp.arange(experts, dtype=jnp.int32)[None, :]).astype(jnp.int32)
    position = jnp.sum((jnp.cumsum(onehot, axis=0) - onehot) * onehot, axis=1)
    slot_index = (flat_ids * capacity + position).reshape(tok_rows, routes)
    token_of = jnp.repeat(jnp.arange(tok_rows, dtype=jnp.int32), routes)
    slot_token = (
        jnp.zeros((experts * capacity,), jnp.int32).at[slot_index.reshape(-1)].set(token_of)
    )
    hidden_local = gate_served.shape[2]
    col_width = d_model // lax.axis_size("tp")
    own_cols = lax.dynamic_slice_in_dim(normed, lax.axis_index("tp") * col_width, col_width, 1)
    arrived = lax.all_to_all(own_cols[slot_token], "fs", split_axis=0, concat_axis=0, tiled=True)
    arrived = arrived.reshape(sources, per_device, capacity, col_width)
    segment = lax.all_gather(arrived, "tp", axis=3, tiled=True)
    gate_more = jnp.einsum(
        "secd,edh->sech", segment, gate_served, preferred_element_type=jnp.float32
    )
    up_more = jnp.einsum("secd,edh->sech", segment, up_served, preferred_element_type=jnp.float32)
    input_scale = d_model ** (-0.5)
    hidden = (jax.nn.silu(gate_more * input_scale) * (up_more * input_scale)).astype(jnp.bfloat16)
    hidden_scale = (hidden_local * lax.axis_size("tp")) ** (-0.5)
    slots_here = sources * per_device * capacity
    partial_value = jnp.einsum(
        "edh,sech->dsec", down_served, hidden, preferred_element_type=jnp.float32
    )
    summed = lax.psum_scatter(
        (
            partial_value.reshape(
                lax.axis_size("tp") * (d_model // lax.axis_size("tp")), slots_here
            )
            * hidden_scale
        ).astype(jnp.bfloat16),
        "tp",
        scatter_dimension=0,
        tiled=True,
    )
    returned = lax.all_to_all(summed, "fs", split_axis=1, concat_axis=1, tiled=True)
    picked = jnp.take(returned, slot_index, axis=1).astype(jnp.float32)
    combined = jnp.einsum("dtk,tk->td", picked, route_weights, precision=lax.Precision.HIGHEST)
    return (gate_served, up_served, down_served, combined.astype(jnp.bfloat16))


def solution(mesh):
    placed = (
        P("fs", None),
        P("fs", None),
        P("fs", None),
        P("fs"),
        P(None, "fs", "tp"),
        P(None, "fs", "tp"),
        P(None, "fs", "tp"),
    )
    return jax.shard_map(
        body,
        mesh=mesh,
        in_specs=placed,
        out_specs=(P("fs", None, "tp"), P("fs", None, "tp"), P("fs", None, "tp"), P("fs", "tp")),
        check_vma=False,
    )
```

profile of v0, /device:TPU:0, one launch (start us, length us, event | category | flops | bytes accessed | tf_op | source)
XLA Modules:
  0.0 264.3 jit_solution(7585327871721887649)
XLA Ops:
  7.2 1.1 convert_element_type.43
  8.3 1.2 multiply_reduce_fusion
  11.3 1.4 scatter_custom_fusion
  12.9 2.6 gather_fusion
  15.5 7.3 %all-to-all-start.3 = ((bf16[8,64,512]{2,1,0:T(8,128)(2,1)}), bf16[8,64,512]{2,1,0:T(8,128)(2,1)S(1)}, u32[]{:S(2)}, u32[]{:S(2)}) async-start(bf16[8,64,512]{2,1,0:T(8,128)(2,1)} %bitcast.15), calls=%async_computation.3 | async-start | bytes 1048576 | tf_op jit(solution)/shard_map/all_to_all | solution.py:41
  22.8 5.8 %multiply_convert_fusion.1 = (bf16[16,256,256]{2,1,0:T(8,128)(2,1)}, bf16[16,256,256]{2,1,0:T(8,128)(2,1)S(1)}) fusion(f32[16,256,256]{2,1,0:T(8,128)} %param.12, f32[256]{0:T(256)S(1)} %copy-done.3, f32[16,256,256]{2,1,0:T(8,128)} %param.11), kind=kLoop, calls=%fused_computation.4 | loop fusion | flops 4194304 | bytes 12583936 | tf_op jit(solution)/shard_map/convert_element_type | solution.py:13
  28.6 8.7 %all-to-all-done.3 = bf16[8,64,512]{2,1,0:T(8,128)(2,1)S(1)} async-done(((bf16[8,64,512]{2,1,0:T(8,128)(2,1)}), bf16[8,64,512]{2,1,0:T(8,128)(2,1)S(1)}, u32[]{:S(2)}, u32[]{:S(2)}) %all-to-all-start.3) | async-done | bytes 524320 | tf_op jit(solution)/shard_map/all_to_all | solution.py:41
  37.3 51.9 %all_to_all.75 = bf16[16,256,256]{2,1,0:T(8,128)(2,1)} all-to-all(bf16[16,256,256]{2,1,0:T(8,128)(2,1)S(1)} %get-tuple-element.7), channel_id=1, replica_groups=mesh['fs'=8,'tp'=4] {'fs'}, dimensions={0} | all-to-all | bytes 4194304 | tf_op jit(solution)/shard_map/all_to_all | solution.py:16
  89.2 4.3 %all-to-all-start.1 = ((bf16[16,256,256]{2,1,0:T(8,128)(2,1)}), bf16[16,256,256]{2,1,0:T(8,128)(2,1)}, u32[]{:S(2)}, u32[]{:S(2)}) async-start(bf16[16,256,256]{2,1,0:T(8,128)(2,1)} %get-tuple-element.6), calls=%async_computation.1 | async-start | bytes 4194304 | tf_op jit(solution)/shard_map/all_to_all | solution.py:17
  93.5 3.8 %convert_element_type.40 = bf16[16,256,256]{2,1,0:T(8,128)(2,1)} convert(f32[16,256,256]{2,1,0:T(8,128)} %param.13) | non-fusion elementwise | flops 1048576 | bytes 6291456 | tf_op jit(solution)/shard_map/convert_element_type | solution.py:14
  97.3 43.5 %all-to-all-done.1 = bf16[16,256,256]{2,1,0:T(8,128)(2,1)} async-done(((bf16[16,256,256]{2,1,0:T(8,128)(2,1)}), bf16[16,256,256]{2,1,0:T(8,128)(2,1)}, u32[]{:S(2)}, u32[]{:S(2)}) %all-to-all-start.1) | async-done | bytes 2097184 | tf_op jit(solution)/shard_map/all_to_all | solution.py:17
  140.8 4.4 %all-to-all-start.2 = ((bf16[16,256,256]{2,1,0:T(8,128)(2,1)}), bf16[16,256,256]{2,1,0:T(8,128)(2,1)}, u32[]{:S(2)}, u32[]{:S(2)}) async-start(bf16[16,256,256]{2,1,0:T(8,128)(2,1)} %convert_element_type.40), calls=%async_computation.2 | async-start | bytes 4194304 | tf_op jit(solution)/shard_map/all_to_all | solution.py:18
  146.2 1.5 copy.24
  147.6 3.1 %copy.25 = bf16[8,2,256,256]{3,2,0,1:T(8,128)(2,1)} copy(bf16[8,2,256,256]{3,2,1,0:T(8,128)(2,1)} %bitcast.3) | data formatting | bytes 4194304 | tf_op jit(solution)/shard_map/all_to_all | solution.py:17
  150.7 42.2 %all-to-all-done.2 = bf16[16,256,256]{2,1,0:T(8,128)(2,1)} async-done(((bf16[16,256,256]{2,1,0:T(8,128)(2,1)}), bf16[16,256,256]{2,1,0:T(8,128)(2,1)}, u32[]{:S(2)}, u32[]{:S(2)}) %all-to-all-start.2) | async-done | bytes 2097184 | tf_op jit(solution)/shard_map/all_to_all | solution.py:18
  193.0 3.2 %copy.26 = bf16[8,2,256,256]{3,2,0,1:T(8,128)(2,1)} copy(bf16[8,2,256,256]{3,2,1,0:T(8,128)(2,1)} %bitcast.6) | data formatting | bytes 4194304 | tf_op jit(solution)/shard_map/all_to_all | solution.py:18
  196.2 2.3 fusion.3
  198.5 4.2 %fusion = bf16[2048,8,2,32]{0,3,1,2:T(8,128)(2,1)S(1)} fusion(bf16[2,2048,256,1]{2,1,3,0:T(8,128)(2,1)} %bitcast.82, bf16[2,2048,256,1]{2,1,3,0:T(8,128)(2,1)} %bitcast.80, bf16[8,2,32,2048]{3,2,0,1:T(8,128)(2,1)} %all-gather.2.cloned.1.call-done, f32[8,2,32,256]{3,2,0,1:T(8,128)S(1)} %fusion.3), kind=kOutput, calls=%fused_computation.6 | convolution fusion | flops 1076756480 | bytes 8912896 | tf_op jit(solution)/shard_map/edh,sech->dsec/dot_general | solution.py:52
  202.8 1.5 copy.34
  204.3 30.4 %reduce-scatter.2.cloned.1.call-done = bf16[512,512]{0,1:T(8,128)(2,1)} async-done(((bf16[2048,512]{0,1:T(8,128)(2,1)}), bf16[512,512]{0,1:T(8,128)(2,1)}) %reduce-scatter.2.cloned.1.call-update) | async-done | bytes 524304 | tf_op jit(solution)/shard_map/reduce_scatter | solution.py:55
  234.6 5.5 %all-to-all-start.4 = ((bf16[512,8,64]{0,2,1:T(8,128)(2,1)}), bf16[512,8,64]{0,2,1:T(8,128)(2,1)S(1)}, u32[]{:S(2)}, u32[]{:S(2)}) async-start(bf16[512,8,64]{0,2,1:T(8,128)(2,1)} %bitcast.85), calls=%async_computation.5 | async-start | bytes 1048576 | tf_op jit(solution)/shard_map/all_to_all | solution.py:66
  240.9 13.6 %all-to-all-done.4 = bf16[512,8,64]{0,2,1:T(8,128)(2,1)S(1)} async-done(((bf16[512,8,64]{0,2,1:T(8,128)(2,1)}), bf16[512,8,64]{0,2,1:T(8,128)(2,1)S(1)}, u32[]{:S(2)}, u32[]{:S(2)}) %all-to-all-start.4) | async-done | bytes 524320 | tf_op jit(solution)/shard_map/all_to_all | solution.py:66
  254.5 1.2 gather_fusion.1
  255.8 1.1 fusion.14
  (45 shorter events, 4.3 us)
Async XLA Ops:
  7.2 2.4 copy-start.2
  12.8 9.9 %copy-start.3 = (f32[256]{0:T(256)S(1)}, f32[256]{0:T(256)}, u32[]{:S(2)}) copy-start(f32[256]{0:T(256)} %param.10) | copy-start | bytes 3076
  15.5 21.8 %all-to-all-start.3 = ((bf16[8,64,512]{2,1,0:T(8,128)(2,1)}), bf16[8,64,512]{2,1,0:T(8,128)(2,1)S(1)}, u32[]{:S(2)}, u32[]{:S(2)}) async-start(bf16[8,64,512]{2,1,0:T(8,128)(2,1)} %bitcast.15), calls=%async_computation.3 | async-start | bytes 1048576 | tf_op jit(solution)/shard_map/all_to_all | solution.py:41
  89.2 51.6 %all-to-all-start.1 = ((bf16[16,256,256]{2,1,0:T(8,128)(2,1)}), bf16[16,256,256]{2,1,0:T(8,128)(2,1)}, u32[]{:S(2)}, u32[]{:S(2)}) async-start(bf16[16,256,256]{2,1,0:T(8,128)(2,1)} %get-tuple-element.6), calls=%async_computation.1 | async-start | bytes 4194304 | tf_op jit(solution)/shard_map/all_to_all | solution.py:17
  97.3 48.8 %copy-start = (bf16[16,256,256]{2,1,0:T(8,128)(2,1)S(1)}, bf16[16,256,256]{2,1,0:T(8,128)(2,1)}, u32[]{:S(2)}) copy-start(bf16[16,256,256]{2,1,0:T(8,128)(2,1)} %all_to_all.75) | copy-start | bytes 6291460
  140.8 52.2 %all-to-all-start.2 = ((bf16[16,256,256]{2,1,0:T(8,128)(2,1)}), bf16[16,256,256]{2,1,0:T(8,128)(2,1)}, u32[]{:S(2)}, u32[]{:S(2)}) async-start(bf16[16,256,256]{2,1,0:T(8,128)(2,1)} %convert_element_type.40), calls=%async_computation.2 | async-start | bytes 4194304 | tf_op jit(solution)/shard_map/all_to_all | solution.py:18
  145.2 51.0 %all-gather.2.cloned.1.call-start = ((), (), s32[]{:S(2)}) async-start(), calls=%async_computation.6 | async-start | bytes 2621440 | tf_op jit(solution)/shard_map/all_gather | solution.py:43
  146.1 88.5 %reduce-scatter.2.cloned.1.call-start = ((), (), s32[]{:S(2)}) async-start(), calls=%async_computation.7 | async-start | bytes 2621440 | tf_op jit(solution)/shard_map/reduce_scatter | solution.py:55
  193.0 3.3 %copy-start.1 = (bf16[8,2,256,256]{3,2,0,1:T(8,128)(2,1)S(1)}, bf16[8,2,256,256]{3,2,0,1:T(8,128)(2,1)}, u32[]{:S(2)}) copy-start(bf16[8,2,256,256]{3,2,0,1:T(8,128)(2,1)} %copy.24) | copy-start | bytes 6291460
  204.2 36.5 %copy-start.4 = (f32[128,2]{0,1:T(2,128)S(1)}, f32[128,2]{0,1:T(2,128)}, u32[]{:S(2)}) copy-start(f32[128,2]{0,1:T(2,128)} %param.9) | copy-start | bytes 3076
  234.6 19.8 %all-to-all-start.4 = ((bf16[512,8,64]{0,2,1:T(8,128)(2,1)}), bf16[512,8,64]{0,2,1:T(8,128)(2,1)S(1)}, u32[]{:S(2)}, u32[]{:S(2)}) async-start(bf16[512,8,64]{0,2,1:T(8,128)(2,1)} %bitcast.85), calls=%async_computation.5 | async-start | bytes 1048576 | tf_op jit(solution)/shard_map/all_to_all | solution.py:66
Sparse Core Ops, SparseCore 0:
  147.5 23.8 all-gather.1
  204.4 30.2 reduce-scatter.1
where the time goes:
time: 265 us; the launch traced here: 264 us
  waiting for transfers between devices  138 us (52%)
  blocking collectives  51.9 us (20%)
  starting transfers between devices  21.6 us (8%)
  local copies, waits for them, and re-layouts  17.8 us (7%)
  between operations  14.2 us (5%)
  other arithmetic  12.9 us (5%)
  matrix products  7.6 us (3%)
    all_to_all x1, blocking collectives, body(): lax.all_to_all(gate_folded, 'fs', split_axis=0, concat_axis=1, tiled=True)  51.9 us
    all_to_all x1, waiting for transfers between devices, body(): lax.all_to_all(up_folded, 'fs', split_axis=0, concat_axis=1, tiled=True)  43.5 us
    all_to_all x1, waiting for transfers between devices, body(): lax.all_to_all(down_rounded, 'fs', split_axis=0, concat_axis=1, tiled=True)  42.2 us
    reduce_scatter x1, waiting for transfers between devices, body(): lax.psum_scatter((partial_value.reshape(lax.axis_size('tp') * (d_model //...  30.4 us
    all_to_all x1, waiting for transfers between devices, body(): lax.all_to_all(summed, 'fs', split_axis=1, concat_axis=1, tiled=True)  13.6 us
    all_to_all x1, waiting for transfers between devices, body(): lax.all_to_all(own_cols[slot_token], 'fs', split_axis=0, concat_axis=0, t...  8.67 us
    all_to_all x1, starting transfers between devices, body(): lax.all_to_all(own_cols[slot_token], 'fs', split_axis=0, concat_axis=0, t...  7.28 us
    convert_element_type x1, other arithmetic, body(): up_folded = (scaling * up_weight).astype(jnp.bfloat16)  5.81 us
  transfers between devices with their start and end apart: 6, of which 5 were waited for; matrix products, arithmetic and copies ran while one was open for 7% of the time, Pallas kernels for 0%

commit v1 on v0

--- a/solution.py
+++ b/solution.py
@@ -5,6 +5,18 @@
 
 GROUPS = 4
 epsilon = 1e-06
+
+
+def split_up(shard, dim, peers):
+    dims = shard.shape
+    pieces = shard.reshape(*dims[:dim], peers, dims[dim] // peers, *dims[dim + 1 :])
+    return jnp.moveaxis(pieces, dim, 0)
+
+
+def in_order(blocks, dim):
+    dims = list(blocks.shape[1:])
+    dims[dim] *= blocks.shape[0]
+    return jnp.moveaxis(blocks, 0, dim).reshape(dims)
 
 
 def body(tokens, route_ids, route_weights, norm_gain, gate_weight, up_weight, down_weight):
@@ -38,7 +50,14 @@
     hidden_local = gate_served.shape[2]
     col_width = d_model // lax.axis_size("tp")
     own_cols = lax.dynamic_slice_in_dim(normed, lax.axis_index("tp") * col_width, col_width, 1)
-    arrived = lax.all_to_all(own_cols[slot_token], "fs", split_axis=0, concat_axis=0, tiled=True)
+    size, index = (lax.axis_size("fs"), lax.axis_index("fs"))
+    blocks = split_up(own_cols[slot_token], 0, size)
+    finished = [blocks[index]]
+    for step in range(1, size):
+        sent = blocks[index ^ step]
+        finished.append(lax.ppermute(sent, "fs", [(i, i ^ step) for i in range(size)]))
+    blocks = jnp.stack(finished)[index ^ jnp.arange(size)]
+    arrived = in_order(blocks, 0)
     arrived = arrived.reshape(sources, per_device, capacity, col_width)
     segment = lax.all_gather(arrived, "tp", axis=3, tiled=True)
     gate_more = jnp.einsum(

time: 265 us -> 251 us (0.947)
  waiting for transfers between devices: 138 us -> 113 us
  starting transfers between devices: 21.6 us -> 30.1 us
  blocking collectives: 51.9 us -> 55.3 us
    all_to_all x1, waiting for transfers between devices: 43.5 us -> 0.01 us  [body(): lax.all_to_all(up_folded, 'fs', split_axis=0, concat_axis=1, tiled=True)]
    ppermute x0 -> x7, waiting for transfers between devices: none -> 29.2 us  [body(): lax.ppermute(sent, 'fs', [(i, i ^ step) for i in range(size)])]
    ppermute x0 -> x7, starting transfers between devices: none -> 15.7 us  [body(): lax.ppermute(sent, 'fs', [(i, i ^ step) for i in range(size)])]
    all_to_all x1 -> x0, waiting for transfers between devices: 8.67 us -> none  [body(): lax.all_to_all(own_cols[slot_token], 'fs', split_axis=0, concat_axis=0, t...]
    all_to_all x1 -> x0, starting transfers between devices: 7.28 us -> none  [body(): lax.all_to_all(own_cols[slot_token], 'fs', split_axis=0, concat_axis=0, t...]
    all_to_all x1, blocking collectives: 51.9 us -> 55.3 us  [body(): lax.all_to_all(gate_folded, 'fs', split_axis=0, concat_axis=1, tiled=True)]
  transfers between devices with their start and end apart: 6 -> 12, of which waited for: 5 -> 5; matrix products, arithmetic and copies ran while one was open for 7% -> 8% of each run, Pallas kernels for 0% -> 0%
where the time goes in v1:
time: 251 us
  waiting for transfers between devices  113 us (45%)
  blocking collectives  55.3 us (22%)
  starting transfers between devices  30.1 us (12%)
  local copies, waits for them, and re-layouts  17.8 us (7%)
  between operations  14.4 us (6%)
  other arithmetic  12.7 us (5%)
  matrix products  7.59 us (3%)
    all_to_all x1, blocking collectives, body(): lax.all_to_all(gate_folded, 'fs', split_axis=0, concat_axis=1, tiled=True)  55.3 us
    all_to_all x1, waiting for transfers between devices, body(): lax.all_to_all(down_rounded, 'fs', split_axis=0, concat_axis=1, tiled=True)  39.7 us
    reduce_scatter x1, waiting for transfers between devices, body(): lax.psum_scatter((partial_value.reshape(lax.axis_size('tp') * (d_model //...  30.2 us
    ppermute x7, waiting for transfers between devices, body(): lax.ppermute(sent, 'fs', [(i, i ^ step) for i in range(size)])  29.2 us
    ppermute x7, starting transfers between devices, body(): lax.ppermute(sent, 'fs', [(i, i ^ step) for i in range(size)])  15.7 us
    all_to_all x1, waiting for transfers between devices, body(): lax.all_to_all(summed, 'fs', split_axis=1, concat_axis=1, tiled=True)  13.6 us
    convert_element_type x1, other arithmetic, body(): up_folded = (scaling * up_weight).astype(jnp.bfloat16)  5.83 us
    all_to_all x1, starting transfers between devices, body(): lax.all_to_all(summed, 'fs', split_axis=1, concat_axis=1, tiled=True)  5.48 us
  transfers between devices with their start and end apart: 12, of which 5 were waited for; matrix products, arithmetic and copies ran while one was open for 8% of the time, Pallas kernels for 0%

profile of v1, /device:TPU:0, one launch (start us, length us, event | category | flops | bytes accessed | tf_op | source)
XLA Modules:
  0.0 250.6 jit_solution(5679863571891707232)
XLA Ops:
  7.2 5.8 %multiply_convert_fusion.1 = (bf16[16,256,256]{2,1,0:T(8,128)(2,1)}, bf16[16,256,256]{2,1,0:T(8,128)(2,1)S(1)}) fusion(f32[16,256,256]{2,1,0:T(8,128)} %param.12, f32[256]{0:T(256)} %param.10, f32[16,256,256]{2,1,0:T(8,128)} %param.11), kind=kLoop, calls=%fused_computation.5 | loop fusion | flops 4194304 | bytes 12583936 | tf_op jit(solution)/shard_map/convert_element_type | solution.py:25
  13.0 55.3 %all_to_all.66 = bf16[16,256,256]{2,1,0:T(8,128)(2,1)S(1)} all-to-all(bf16[16,256,256]{2,1,0:T(8,128)(2,1)S(1)} %get-tuple-element.15), channel_id=1, replica_groups=mesh['fs'=8,'tp'=4] {'fs'}, dimensions={0} | all-to-all | bytes 4194304 | tf_op jit(solution)/shard_map/all_to_all | solution.py:28
  68.3 4.5 %all-to-all-start.1 = ((bf16[16,256,256]{2,1,0:T(8,128)(2,1)}), bf16[16,256,256]{2,1,0:T(8,128)(2,1)}, u32[]{:S(2)}, u32[]{:S(2)}) async-start(bf16[16,256,256]{2,1,0:T(8,128)(2,1)} %get-tuple-element.14), calls=%async_computation.1 | async-start | bytes 4194304 | tf_op jit(solution)/shard_map/all_to_all | solution.py:29
  78.4 2.0 gather_fusion
  80.4 1.9 collective-permute-start
  82.3 1.5 collective-permute-start.1
  84.0 2.8 %collective-permute-start.3 = (bf16[64,512]{1,0:T(8,128)(2,1)S(1)}, bf16[64,512]{1,0:T(8,128)(2,1)S(1)}, u32[]{:S(2)}, u32[]{:S(2)}) collective-permute-start(bf16[64,512]{1,0:T(8,128)(2,1)S(1)} %get-tuple-element.9), channel_id=1, source_target_pairs={{0,16},{4,20},{8,24},{12,28},{16,0},{20,4},{24,8},{28,12},{1,17},{... | collective-permute-start | bytes 196616 | tf_op jit(solution)/shard_map/ppermute | solution.py:58
  86.7 1.4 collective-permute-start.4
  88.2 3.8 %convert_element_type.40 = bf16[16,256,256]{2,1,0:T(8,128)(2,1)} convert(f32[16,256,256]{2,1,0:T(8,128)} %param.13) | non-fusion elementwise | flops 1048576 | bytes 6291456 | tf_op jit(solution)/shard_map/convert_element_type | solution.py:26
  92.0 3.4 %collective-permute-start.5 = (bf16[64,512]{1,0:T(8,128)(2,1)S(1)}, bf16[64,512]{1,0:T(8,128)(2,1)S(1)}, u32[]{:S(2)}, u32[]{:S(2)}) collective-permute-start(bf16[64,512]{1,0:T(8,128)(2,1)S(1)} %get-tuple-element.7), channel_id=1, source_target_pairs={{0,24},{4,28},{8,16},{12,20},{16,8},{20,12},{24,0},{28,4},{1,25},{... | collective-permute-start | bytes 196616 | tf_op jit(solution)/shard_map/ppermute | solution.py:58
  95.4 14.0 %collective-permute-done.1 = bf16[64,512]{1,0:T(8,128)(2,1)S(1)} collective-permute-done((bf16[64,512]{1,0:T(8,128)(2,1)S(1)}, bf16[64,512]{1,0:T(8,128)(2,1)S(1)}, u32[]{:S(2)}, u32[]{:S(2)}) %collective-permute-start.1) | collective-permute-done | bytes 65568 | tf_op jit(solution)/shard_map/ppermute | solution.py:58
  109.3 4.6 %collective-permute-start.6 = (bf16[64,512]{1,0:T(8,128)(2,1)S(1)}, bf16[64,512]{1,0:T(8,128)(2,1)S(1)}, u32[]{:S(2)}, u32[]{:S(2)}) collective-permute-start(bf16[64,512]{1,0:T(8,128)(2,1)S(1)} %get-tuple-element.6), channel_id=1, source_target_pairs={{0,28},{4,24},{8,20},{12,16},{16,12},{20,8},{24,4},{28,0},{1,29},{... | collective-permute-start | bytes 196616 | tf_op jit(solution)/shard_map/ppermute | solution.py:58
  113.9 15.2 %collective-permute-done.3 = bf16[64,512]{1,0:T(8,128)(2,1)S(1)} collective-permute-done((bf16[64,512]{1,0:T(8,128)(2,1)S(1)}, bf16[64,512]{1,0:T(8,128)(2,1)S(1)}, u32[]{:S(2)}, u32[]{:S(2)}) %collective-permute-start.3) | collective-permute-done | bytes 65568 | tf_op jit(solution)/shard_map/ppermute | solution.py:58
  129.2 4.4 %all-to-all-start.2 = ((bf16[16,256,256]{2,1,0:T(8,128)(2,1)}), bf16[16,256,256]{2,1,0:T(8,128)(2,1)}, u32[]{:S(2)}, u32[]{:S(2)}) async-start(bf16[16,256,256]{2,1,0:T(8,128)(2,1)} %convert_element_type.40), calls=%async_computation.2 | async-start | bytes 4194304 | tf_op jit(solution)/shard_map/all_to_all | solution.py:30
  135.2 1.5 copy.24
  136.7 3.1 %copy.25 = bf16[8,2,256,256]{3,2,0,1:T(8,128)(2,1)} copy(bf16[8,2,256,256]{3,2,1,0:T(8,128)(2,1)} %bitcast.3) | data formatting | bytes 4194304 | tf_op jit(solution)/shard_map/all_to_all | solution.py:29
  139.8 39.7 %all-to-all-done.2 = bf16[16,256,256]{2,1,0:T(8,128)(2,1)} async-done(((bf16[16,256,256]{2,1,0:T(8,128)(2,1)}), bf16[16,256,256]{2,1,0:T(8,128)(2,1)}, u32[]{:S(2)}, u32[]{:S(2)}) %all-to-all-start.2) | async-done | bytes 2097184 | tf_op jit(solution)/shard_map/all_to_all | solution.py:30
  179.4 3.2 %copy.26 = bf16[8,2,256,256]{3,2,0,1:T(8,128)(2,1)} copy(bf16[8,2,256,256]{3,2,1,0:T(8,128)(2,1)} %bitcast.6) | data formatting | bytes 4194304 | tf_op jit(solution)/shard_map/all_to_all | solution.py:30
  182.7 2.3 fusion.3
  185.0 4.2 %fusion = bf16[2048,8,2,32]{0,3,1,2:T(8,128)(2,1)S(1)} fusion(bf16[2,2048,256,1]{2,1,3,0:T(8,128)(2,1)} %bitcast.113, bf16[2,2048,256,1]{2,1,3,0:T(8,128)(2,1)} %bitcast.111, bf16[8,2,32,2048]{3,2,0,1:T(8,128)(2,1)} %all-gather.2.cloned.1.call-done, f32[8,2,32,256]{3,2,0,1:T(8,128)S(1)} %fusion.3), kind=kOutput, calls=%fused_computation.7 | convolution fusion | flops 1076756480 | bytes 8912896 | tf_op jit(solution)/shard_map/edh,sech->dsec/dot_general | solution.py:71
  189.2 1.5 copy.34
  190.7 30.2 %reduce-scatter.2.cloned.1.call-done = bf16[512,512]{0,1:T(8,128)(2,1)} async-done(((bf16[2048,512]{0,1:T(8,128)(2,1)}), bf16[512,512]{0,1:T(8,128)(2,1)}) %reduce-scatter.2.cloned.1.call-update) | async-done | bytes 524304 | tf_op jit(solution)/shard_map/reduce_scatter | solution.py:74
  220.9 5.5 %all-to-all-start.3 = ((bf16[512,8,64]{0,2,1:T(8,128)(2,1)}), bf16[512,8,64]{0,2,1:T(8,128)(2,1)S(1)}, u32[]{:S(2)}, u32[]{:S(2)}) async-start(bf16[512,8,64]{0,2,1:T(8,128)(2,1)} %bitcast.116), calls=%async_computation.4 | async-start | bytes 1048576 | tf_op jit(solution)/shard_map/all_to_all | solution.py:85
  227.2 13.6 %all-to-all-done.3 = bf16[512,8,64]{0,2,1:T(8,128)(2,1)S(1)} async-done(((bf16[512,8,64]{0,2,1:T(8,128)(2,1)}), bf16[512,8,64]{0,2,1:T(8,128)(2,1)S(1)}, u32[]{:S(2)}, u32[]{:S(2)}) %all-to-all-start.3) | async-done | bytes 524320 | tf_op jit(solution)/shard_map/all_to_all | solution.py:85
  (66 shorter events, 11.0 us)
Async XLA Ops:
  68.3 4.5 %copy-start.2 = (s32[128,2]{0,1:T(2,128)S(1)}, s32[128,2]{0,1:T(2,128)}, u32[]{:S(2)}) copy-start(s32[128,2]{0,1:T(2,128)} %param.8) | copy-start | bytes 3076
  68.3 4.9 %copy-start = (bf16[128,2048]{1,0:T(8,128)(2,1)S(1)}, bf16[128,2048]{1,0:T(8,128)(2,1)}, u32[]{:S(2)}) copy-start(bf16[128,2048]{1,0:T(8,128)(2,1)} %param.7) | copy-start | bytes 1572868
  68.3 60.9 %all-to-all-start.1 = ((bf16[16,256,256]{2,1,0:T(8,128)(2,1)}), bf16[16,256,256]{2,1,0:T(8,128)(2,1)}, u32[]{:S(2)}, u32[]{:S(2)}) async-start(bf16[16,256,256]{2,1,0:T(8,128)(2,1)} %get-tuple-element.14), calls=%async_computation.1 | async-start | bytes 4194304 | tf_op jit(solution)/shard_map/all_to_all | solution.py:29
  80.4 11.6 %collective-permute-start = (bf16[64,512]{1,0:T(8,128)(2,1)S(1)}, bf16[64,512]{1,0:T(8,128)(2,1)S(1)}, u32[]{:S(2)}, u32[]{:S(2)}) collective-permute-start(bf16[64,512]{1,0:T(8,128)(2,1)S(1)} %get-tuple-element.12), channel_id=1, source_target_pairs={{0,4},{4,0},{8,12},{12,8},{16,20},{20,16},{24,28},{28,24},{1,5},{5... | collective-permute-start | bytes 196616 | tf_op jit(solution)/shard_map/ppermute | solution.py:58
  82.3 27.0 %collective-permute-start.1 = (bf16[64,512]{1,0:T(8,128)(2,1)S(1)}, bf16[64,512]{1,0:T(8,128)(2,1)S(1)}, u32[]{:S(2)}, u32[]{:S(2)}) collective-permute-start(bf16[64,512]{1,0:T(8,128)(2,1)S(1)} %get-tuple-element.11), channel_id=1, source_target_pairs={{0,8},{4,12},{8,0},{12,4},{16,24},{20,28},{24,16},{28,20},{1,9},{5... | collective-permute-start | bytes 196616 | tf_op jit(solution)/shard_map/ppermute | solution.py:58
  83.8 30.1 %collective-permute-start.2 = (bf16[64,512]{1,0:T(8,128)(2,1)S(1)}, bf16[64,512]{1,0:T(8,128)(2,1)S(1)}, u32[]{:S(2)}, u32[]{:S(2)}) collective-permute-start(bf16[64,512]{1,0:T(8,128)(2,1)S(1)} %get-tuple-element.10), channel_id=1, source_target_pairs={{0,12},{4,8},{8,4},{12,0},{16,28},{20,24},{24,20},{28,16},{1,13},{... | collective-permute-start | bytes 196616 | tf_op jit(solution)/shard_map/ppermute | solution.py:58
  84.0 45.2 %collective-permute-start.3 = (bf16[64,512]{1,0:T(8,128)(2,1)S(1)}, bf16[64,512]{1,0:T(8,128)(2,1)S(1)}, u32[]{:S(2)}, u32[]{:S(2)}) collective-permute-start(bf16[64,512]{1,0:T(8,128)(2,1)S(1)} %get-tuple-element.9), channel_id=1, source_target_pairs={{0,16},{4,20},{8,24},{12,28},{16,0},{20,4},{24,8},{28,12},{1,17},{... | collective-permute-start | bytes 196616 | tf_op jit(solution)/shard_map/ppermute | solution.py:58
  86.7 46.9 %collective-permute-start.4 = (bf16[64,512]{1,0:T(8,128)(2,1)S(1)}, bf16[64,512]{1,0:T(8,128)(2,1)S(1)}, u32[]{:S(2)}, u32[]{:S(2)}) collective-permute-start(bf16[64,512]{1,0:T(8,128)(2,1)S(1)} %get-tuple-element.8), channel_id=1, source_target_pairs={{0,20},{4,16},{8,28},{12,24},{16,4},{20,0},{24,12},{28,8},{1,21},{... | collective-permute-start | bytes 196616 | tf_op jit(solution)/shard_map/ppermute | solution.py:58
  92.0 41.6 %collective-permute-start.5 = (bf16[64,512]{1,0:T(8,128)(2,1)S(1)}, bf16[64,512]{1,0:T(8,128)(2,1)S(1)}, u32[]{:S(2)}, u32[]{:S(2)}) collective-permute-start(bf16[64,512]{1,0:T(8,128)(2,1)S(1)} %get-tuple-element.7), channel_id=1, source_target_pairs={{0,24},{4,28},{8,16},{12,20},{16,8},{20,12},{24,0},{28,4},{1,25},{... | collective-permute-start | bytes 196616 | tf_op jit(solution)/shard_map/ppermute | solution.py:58
  109.3 24.3 %collective-permute-start.6 = (bf16[64,512]{1,0:T(8,128)(2,1)S(1)}, bf16[64,512]{1,0:T(8,128)(2,1)S(1)}, u32[]{:S(2)}, u32[]{:S(2)}) collective-permute-start(bf16[64,512]{1,0:T(8,128)(2,1)S(1)} %get-tuple-element.6), channel_id=1, source_target_pairs={{0,28},{4,24},{8,20},{12,16},{16,12},{20,8},{24,4},{28,0},{1,29},{... | collective-permute-start | bytes 196616 | tf_op jit(solution)/shard_map/ppermute | solution.py:58
  129.2 50.3 %all-to-all-start.2 = ((bf16[16,256,256]{2,1,0:T(8,128)(2,1)}), bf16[16,256,256]{2,1,0:T(8,128)(2,1)}, u32[]{:S(2)}, u32[]{:S(2)}) async-start(bf16[16,256,256]{2,1,0:T(8,128)(2,1)} %convert_element_type.40), calls=%async_computation.2 | async-start | bytes 4194304 | tf_op jit(solution)/shard_map/all_to_all | solution.py:30
  133.5 49.2 %all-gather.2.cloned.1.call-start = ((), (), s32[]{:S(2)}) async-start(), calls=%async_computation.5 | async-start | bytes 2621440 | tf_op jit(solution)/shard_map/all_gather | solution.py:62
  135.1 85.8 %reduce-scatter.2.cloned.1.call-start = ((), (), s32[]{:S(2)}) async-start(), calls=%async_computation.6 | async-start | bytes 2621440 | tf_op jit(solution)/shard_map/reduce_scatter | solution.py:74
  179.4 3.3 %copy-start.1 = (bf16[8,2,256,256]{3,2,0,1:T(8,128)(2,1)S(1)}, bf16[8,2,256,256]{3,2,0,1:T(8,128)(2,1)}, u32[]{:S(2)}) copy-start(bf16[8,2,256,256]{3,2,0,1:T(8,128)(2,1)} %copy.24) | copy-start | bytes 6291460
  190.7 36.3 %copy-start.3 = (f32[128,2]{0,1:T(2,128)S(1)}, f32[128,2]{0,1:T(2,128)}, u32[]{:S(2)}) copy-start(f32[128,2]{0,1:T(2,128)} %param.9) | copy-start | bytes 3076
  220.9 19.8 %all-to-all-start.3 = ((bf16[512,8,64]{0,2,1:T(8,128)(2,1)}), bf16[512,8,64]{0,2,1:T(8,128)(2,1)S(1)}, u32[]{:S(2)}, u32[]{:S(2)}) async-start(bf16[512,8,64]{0,2,1:T(8,128)(2,1)} %bitcast.116), calls=%async_computation.4 | async-start | bytes 1048576 | tf_op jit(solution)/shard_map/all_to_all | solution.py:85
Sparse Core Ops, SparseCore 0:
  135.9 23.8 all-gather.1
  190.9 30.0 reduce-scatter.1
